TPU v7x, 32 devices: a whole 2x2x4 slice. The times are simulated.
32 devices in a mesh: sp: 8 (over z, y), tp: 4 (over x, core).
Axes of the slice: x: 2, y: 2, z: 4, core: 2. Of those that a mesh axis runs over, the one named last changes fastest.
Arguments:
- resid: bfloat16 [2048, 2048], P(('sp', 'tp')), may hold values from -0.3125 to 0.3125
- q_latent: bfloat16 [2048, 768], P('sp'), may hold values from -6 to 6
- kv_latent: bfloat16 [2048, 512], P('sp'), may hold values from -6 to 6
- rope_key: bfloat16 [2048, 32], P('sp'), may hold values from -6 to 6
- q_gain: float32 [768], replicated, may hold values from 0.6 to 10, as said below
- kv_gain: float32 [512], replicated, may hold values from 0.6 to 10
- w_q_small: bfloat16 [768, 768], P(None, 'tp'), may hold values from -0.21875 to 0.21875
- w_q_large: bfloat16 [768, 1280], P(None, 'tp'), may hold values from -0.21875 to 0.21875
- w_kv_small: bfloat16 [512, 1024], P(None, 'tp'), may hold values from -0.25 to 0.25
- w_kv_large: bfloat16 [512, 2048], P(None, 'tp'), may hold values from -0.25 to 0.25
- w_out_small: bfloat16 [512, 2048], P('tp'), may hold values from -0.15625 to 0.15625
- w_out_large: bfloat16 [1024, 2048], P('tp'), may hold values from -0.15625 to 0.15625
- ffn_gain: float32 [2048], replicated, may hold values from 0.1 to 1.9
- w_up: bfloat16 [2048, 8192], P('sp', 'tp'), may hold values from -0.125 to 0.125
- w_down: bfloat16 [8192, 2048], P('tp', 'sp'), may hold values from -0.0625 to 0.0625
Outputs:
- layer_out: bfloat16 [2048, 2048], P(('sp', 'tp'))
Inputs may be any that keep to these rules, and one draw needn't show every extreme that they name: q_gain and kv_gain are positive.
All inputs are finite; a program needn't handle non-finite values.
Results may differ from a plain program's by a relative error of at most 0.025.
The roundings to bfloat16 on the way count: a program that leaves them out, or rounds other values in their place, can miss the bound.
Values may be sent and summed in bfloat16 or wider, within the bound.
A program may use at most 128 MiB of HBM per device.

v0:
```python
import math

import jax
import jax.numpy as jnp
from jax import lax
from jax.sharding import PartitionSpec as P

SMALL_DIM = 64
LARGE_DIM = 128
ROPE_DIM = 32


epsilon = 1e-06
theta_base = 10000.0
mask_floor = -1e30


def rms_scale(inputs, gain_vec):
    values = inputs.astype(jnp.float32)
    return (
        values * lax.rsqrt(jnp.mean(values * values, axis=-1, keepdims=True) + epsilon) * gain_vec
    )


def rotary(values, positions):
    halfway = values.shape[-1] // 2
    inverse = theta_base ** (-jnp.arange(0, 2 * halfway, 2, dtype=jnp.float32) / (2 * halfway))
    angles = positions.astype(jnp.float32)[:, None] * inverse[None, :]
    cos_table = jnp.cos(angles)
    sin_table = jnp.sin(angles)
    if values.ndim == 3:
        cos_table = cos_table[:, None, :]
        sin_table = sin_table[:, None, :]
    first_half = values[..., :halfway]
    second_half = values[..., halfway:]
    return jnp.concatenate(
        [
            first_half * cos_table - second_half * sin_table,
            second_half * cos_table + first_half * sin_table,
        ],
        axis=-1,
    )


def queries(normed, weight, nope_dim, positions):
    projected = jnp.dot(normed, weight, preferred_element_type=jnp.float32)
    projected = projected.reshape(projected.shape[0], -1, nope_dim + ROPE_DIM)
    turned = rotary(projected[..., nope_dim:], positions)
    return jnp.concatenate([projected[..., :nope_dim], turned], axis=-1).astype(jnp.bfloat16)


def update_group(
    running, query_rows, key_block, value_block, key_rot, query_pos, key_pos, nope_dim
):
    row_max, row_sum, weighted = running
    score_scale = query_rows.shape[-1] ** (-0.5)
    scores = jnp.einsum(
        "qhd,khd->hqk", query_rows[..., :nope_dim], key_block, preferred_element_type=jnp.float32
    )
    scores = scores + jnp.einsum(
        "qhr,kr->hqk", query_rows[..., nope_dim:], key_rot, preferred_element_type=jnp.float32
    )
    scores = scores * score_scale
    causal = (key_pos[None, :] <= query_pos[:, None])[None]
    masked = jnp.where(causal, scores, mask_floor)
    new_max = jnp.maximum(row_max, jnp.max(masked, axis=-1))
    shrink = jnp.exp(row_max - new_max)
    weights = jnp.where(causal, jnp.exp(masked - new_max[..., None]), 0.0)
    row_sum = row_sum * shrink + jnp.sum(weights, axis=-1)
    weighted = weighted * shrink[..., None] + jnp.einsum(
        "hqk,khd->hqd",
        weights.astype(jnp.bfloat16),
        value_block,
        preferred_element_type=jnp.float32,
    )
    return (new_max, row_sum, weighted)


def fetch_weights(w_up, w_down):
    return (
        lax.all_gather(w_up, "sp", axis=0, tiled=True),
        lax.all_gather(w_down, "sp", axis=1, tiled=True),
    )


def on_device(
    resid,
    q_latent,
    kv_latent,
    rope_key,
    q_gain,
    kv_gain,
    w_q_small,
    w_q_large,
    w_kv_small,
    w_kv_large,
    w_out_small,
    w_out_large,
    ffn_gain,
    w_up,
    w_down,
):
    tok_rows = q_latent.shape[0]
    offset = lax.axis_index("sp") * tok_rows
    positions = offset + jnp.arange(tok_rows, dtype=jnp.int32)
    last_query = offset + tok_rows - 1
    query_normed = rms_scale(q_latent, q_gain).astype(jnp.bfloat16)
    query_small = queries(query_normed, w_q_small, SMALL_DIM, positions)
    query_large = queries(query_normed, w_q_large, LARGE_DIM, positions)
    key_normed = rms_scale(kv_latent, kv_gain).astype(jnp.bfloat16)
    key_rotated = rotary(rope_key.astype(jnp.float32), positions).astype(jnp.bfloat16)
    small_heads = query_small.shape[1]
    large_heads = query_large.shape[1]

    def empty_state(head_count, head_width):
        return (
            jnp.full((head_count, tok_rows), mask_floor, jnp.float32),
            jnp.zeros((head_count, tok_rows), jnp.float32),
            jnp.zeros((head_count, tok_rows, head_width), jnp.float32),
        )

    initial = (empty_state(small_heads, SMALL_DIM), empty_state(large_heads, LARGE_DIM))

    def from_latent(block_parts):
        latent_block, rot_block = block_parts
        small_kv = jnp.dot(latent_block, w_kv_small, preferred_element_type=jnp.float32).astype(
            jnp.bfloat16
        )
        large_kv = jnp.dot(latent_block, w_kv_large, preferred_element_type=jnp.float32).astype(
            jnp.bfloat16
        )
        return (small_kv, large_kv, rot_block)

    folded = initial
    pieces = (
        lax.all_gather(key_normed, "sp", axis=0, tiled=True),
        lax.all_gather(key_rotated, "sp", axis=0, tiled=True),
    )
    piece_rows = pieces[0].shape[0]
    block_rows = math.gcd(piece_rows, 512)
    block_count = piece_rows // block_rows
    blocked = tuple((p.reshape(block_count, block_rows, p.shape[1]) for p in pieces))

    def key_step(running, block_args):
        block_parts, block_index = block_args
        key_pos = block_index * block_rows + jnp.arange(block_rows, dtype=jnp.int32)

        def attend(state):
            small_kv, large_kv, rot_block = from_latent(block_parts)
            small_kv = small_kv.reshape(block_rows, small_heads, 2 * SMALL_DIM)
            large_kv = large_kv.reshape(block_rows, large_heads, 2 * LARGE_DIM)
            small_state = update_group(
                state[0],
                query_small,
                small_kv[..., :SMALL_DIM],
                small_kv[..., SMALL_DIM:],
                rot_block,
                positions,
                key_pos,
                SMALL_DIM,
            )
            large_state = update_group(
                state[1],
                query_large,
                large_kv[..., :LARGE_DIM],
                large_kv[..., LARGE_DIM:],
                rot_block,
                positions,
                key_pos,
                LARGE_DIM,
            )
            return (small_state, large_state)

        def unchanged(state):
            return state

        running = lax.cond(key_pos[0] <= last_query, attend, unchanged, running)
        return (running, None)

    folded, unused = lax.scan(key_step, folded, (blocked, jnp.arange(block_count, dtype=jnp.int32)))

    def finish(running):
        row_max, row_sum, weighted = running
        normalized = weighted / row_sum[..., None]
        return jnp.transpose(normalized, (1, 0, 2)).reshape(tok_rows, -1).astype(jnp.bfloat16)

    attn_small = finish(folded[0])
    attn_large = finish(folded[1])
    mixed_rows = lax.psum_scatter(
        (
            jnp.dot(attn_small, w_out_small, preferred_element_type=jnp.float32)
            + jnp.dot(attn_large, w_out_large, preferred_element_type=jnp.float32)
        ).astype(jnp.bfloat16),
        "tp",
        scatter_dimension=0,
        tiled=True,
    ).astype(jnp.float32)
    after_attn = (resid.astype(jnp.float32) + mixed_rows).astype(jnp.bfloat16)
    ffn_normed = rms_scale(after_attn, ffn_gain).astype(jnp.bfloat16)
    up_full, down_full = fetch_weights(w_up, w_down)
    projected = jnp.dot(
        lax.all_gather(ffn_normed, "tp", axis=0, tiled=True),
        up_full,
        preferred_element_type=jnp.float32,
    )
    hidden = jnp.square(jax.nn.relu(projected)).astype(jnp.bfloat16)
    ffn_rows = lax.psum_scatter(
        jnp.dot(hidden, down_full, preferred_element_type=jnp.float32).astype(jnp.bfloat16),
        "tp",
        scatter_dimension=0,
        tiled=True,
    ).astype(jnp.float32)
    return (after_attn.astype(jnp.float32) + ffn_rows).astype(jnp.bfloat16)


def solution(mesh):
    return jax.shard_map(
        on_device,
        mesh=mesh,
        in_specs=(
            P(("sp", "tp"), None),
            P("sp", None),
            P("sp", None),
            P("sp", None),
            P(),
            P(),
            P(None, "tp"),
            P(None, "tp"),
            P(None, "tp"),
            P(None, "tp"),
            P("tp", None),
            P("tp", None),
            P(),
            P("sp", "tp"),
            P("tp", "sp"),
        ),
        out_specs=P(("sp", "tp"), None),
        check_vma=False,
    )
```

profile of v0, /device:TPU:0, one launch (start us, length us, event | category | flops | bytes accessed | tf_op | source)
XLA Modules:
  0.0 472.0 jit_solution(17594482973844350327)
XLA Ops:
  6.6 1.2 fusion.48
  7.8 1.8 fusion.50
  9.7 0.7 convert_element_type.105
  10.4 1.2 fusion.45
  11.6 1.6 fusion.55
  14.0 32.9 %all_gather.16 = bf16[2048,32]{0,1:T(8,128)(2,1)S(1)} all-gather(bf16[256,32]{0,1:T(8,128)(2,1)S(1)} %pad_maximum_fusion.2), channel_id=1, replica_groups=mesh['sp'=8,'tp'=4] {'sp'}, dimensions={0}, use_global_device_ids=true | all-gather | bytes 147456 | tf_op jit(solution)/shard_map/all_gather | solution.py:137
  46.8 0.7 copy.60
  47.5 0.6 pad_maximum_fusion.1
  48.1 13.7 %all-gather.5.cloned.1.call-done = bf16[2048,512]{1,0:T(8,128)(2,1)} async-done(((bf16[256,512]{1,0:T(8,128)(2,1)}), bf16[2048,512]{1,0:T(8,128)(2,1)}) %all-gather.5.cloned.1.call-update) | async-done | bytes 2097168 | tf_op jit(solution)/shard_map/all_gather | solution.py:136
  61.8 0.5 iota.18
  62.3 0.7 broadcast_in_dim.68
  63.1 0.6 broadcast_in_dim.47
  63.7 0.6 broadcast.141.clone
  64.3 25.6 %while.21 = (s32[]{:T(128)}, f32[2,256]{1,0:T(2,128)S(1)}, f32[2,256]{1,0:T(2,128)S(1)}, f32[2,256,64]{1,2,0:T(8,128)}, f32[2,256]{1,0:T(2,128)S(1)}, /*index=5*...) while((s32[]{:T(128)}, f32[2,256]{1,0:T(2,128)S(1)}, ...), condition=%wide.region_9.10_spmd.clone, body=%wide.region_2.9_spmd.clone.sunk | while | flops 643500800 | bytes 17639932 | solution.py:180
  64.3 1.3 dynamic_slice.44
  66.3 0.6 slice.134
  67.5 12.6 %conditional.3 = ((f32[2,256]{1,0:T(2,128)S(1)}, f32[2,256]{1,0:T(2,128)S(1)}, f32[2,256,64]{1,2,0:T(8,128)}, f32[2,256]{1,0:T(2,128)S(1)}, f32[2,256]{1,0:T(2,128)}, /*index=5*/f32[2,256,128]{2,1,0:T(8,128)})) conditional(s32[]{:T(128)} %convert_element_type.194, (f32[2,256]{1,0:T(2,128)S(1)}, f32[2,256]{1,0:T(2,128)S(1)}, f32[2,256,64]{1,2,0:T(8,128)}, ...), branch_computations={%region_3.3_spmd, %region_4.8_spmd} | conditional | flops 643500288 | bytes 17636468 | solution.py:177
  67.5 1.5 convolution_convert_fusion
  69.6 0.8 copy.48
  70.4 1.2 fusion.61
  71.6 1.4 convolution_convert_fusion.1
  73.4 1.1 fusion.60
  74.5 0.4 fusion.11
  74.9 1.3 multiply_add_fusion
  76.2 2.1 convolution_add_fusion
  78.3 1.9 convolution_add_fusion.1
  80.2 1.3 dynamic_slice.44
  82.1 0.6 slice.134
  83.4 1.3 dynamic_slice.44
  85.4 0.6 slice.134
  86.7 1.3 dynamic_slice.44
  88.6 0.6 slice.134
  89.9 1.1 copy.53
  91.0 0.7 divide_convert_fusion
  91.7 0.9 divide_convert_fusion.1
  92.6 1.5 fusion.62
  94.2 1.4 fusion.44
  95.7 61.7 %reduce-scatter.3.cloned.1.call-done = bf16[64,2048]{1,0:T(8,128)(2,1)} async-done(((bf16[256,2048]{1,0:T(8,128)(2,1)}), bf16[64,2048]{1,0:T(8,128)(2,1)}) %reduce-scatter.3.cloned.1.call-update) | async-done | bytes 262160 | tf_op jit(solution)/shard_map/reduce_scatter | solution.py:189
  157.4 1.1 fusion.51
  158.6 1.8 fusion.53
  160.4 0.5 all-gather.11.cloned.1.call-update
  161.0 0.5 all-gather.9.cloned.1.call-update
  161.6 15.6 %all-gather.7.cloned.1.call-done = bf16[256,2048]{1,0:T(8,128)(2,1)} async-done(((bf16[64,2048]{1,0:T(8,128)(2,1)}), bf16[256,2048]{1,0:T(8,128)(2,1)}) %all-gather.7.cloned.1.call-update) | async-done | bytes 1048592 | tf_op jit(solution)/shard_map/all_gather | solution.py:202
  177.2 126.9 %all-gather.11.cloned.1.call-done = bf16[2048,2048]{1,0:T(8,128)(2,1)} async-done(((bf16[2048,256]{1,0:T(8,128)(2,1)}), bf16[2048,2048]{1,0:T(8,128)(2,1)}) %all-gather.11.cloned.1.call-update) | async-done | bytes 8388624 | tf_op jit(solution)/shard_map/all_gather | solution.py:82
  304.1 124.7 %all-gather.9.cloned.1.call-done = bf16[2048,2048]{1,0:T(8,128)(2,1)} async-done(((bf16[256,2048]{1,0:T(8,128)(2,1)}), bf16[2048,2048]{1,0:T(8,128)(2,1)}) %all-gather.9.cloned.1.call-update) | async-done | bytes 8388624 | tf_op jit(solution)/shard_map/all_gather | solution.py:81
  428.7 11.5 %convolution_convert_fusion.2 = bf16[256,2048]{1,0:T(8,128)(2,1)} fusion(bf16[2048,2048]{1,0:T(8,128)(2,1)} %all-gather.11.cloned.1.call-done, bf16[256,2048]{1,0:T(8,128)(2,1)} %all-gather.7.cloned.1.call-done, bf16[2048,2048]{1,0:T(8,128)(2,1)} %all-gather.9.cloned.1.call-done), kind=kOutput, calls=%fused_computation.61 | convolution fusion | flops 4297064448 | bytes 18874368 | tf_op jit(solution)/shard_map/dot_general | solution.py:208
  440.3 23.1 %reduce-scatter.5.cloned.1.call-done = bf16[64,2048]{1,0:T(8,128)(2,1)} async-done(((bf16[256,2048]{1,0:T(8,128)(2,1)}), bf16[64,2048]{1,0:T(8,128)(2,1)}) %reduce-scatter.5.cloned.1.call-update) | async-done | bytes 262160 | tf_op jit(solution)/shard_map/reduce_scatter | solution.py:207
  463.4 1.7 fusion.54
  (65 shorter events, 2.0 us)
Async XLA Ops:
  6.5 87.6 %copy-start = (bf16[256,2048]{1,0:T(8,128)(2,1)S(1)}, bf16[256,2048]{1,0:T(8,128)(2,1)}, u32[]{:S(2)}) copy-start(bf16[256,2048]{1,0:T(8,128)(2,1)} %param.30) | copy-start | bytes 3145732
  6.5 6.6 %copy-start.6 = (bf16[256,768]{1,0:T(8,128)(2,1)S(1)}, bf16[256,768]{1,0:T(8,128)(2,1)}, u32[]{:S(2)}) copy-start(bf16[256,768]{1,0:T(8,128)(2,1)} %param.20) | copy-start | bytes 1179652
  6.5 6.6 %copy-start.9 = (f32[768]{0:T(1024)S(1)}, f32[768]{0:T(1024)}, u32[]{:S(2)}) copy-start(f32[768]{0:T(1024)} %param.23) | copy-start | bytes 9220
  6.5 6.6 %copy-start.8 = (bf16[768,192]{0,1:T(8,128)(2,1)S(1)}, bf16[768,192]{0,1:T(8,128)(2,1)}, u32[]{:S(2)}) copy-start(bf16[768,192]{0,1:T(8,128)(2,1)} %param.25) | copy-start | bytes 884740
  6.5 55.3 %all-gather.5.cloned.1.call-start = ((), (), s32[]{:S(2)}) async-start(), calls=%async_computation.2 | async-start | bytes 2359296 | tf_op jit(solution)/shard_map/all_gather | solution.py:136
  9.6 147.8 %reduce-scatter.3.cloned.1.call-start = ((), (), s32[]{:S(2)}) async-start(), calls=%async_computation.3 | async-start | bytes 1310720 | tf_op jit(solution)/shard_map/reduce_scatter | solution.py:189
  13.1 51.2 %copy-start.1 = (bf16[512,512]{1,0:T(8,128)(2,1)S(1)}, bf16[512,512]{1,0:T(8,128)(2,1)}, u32[]{:S(2)}) copy-start(bf16[512,512]{1,0:T(8,128)(2,1)} %param.28) | copy-start | bytes 1572868
  70.4 1.2 copy-start.2
  70.4 2.6 copy-start.3
  94.1 63.3 %copy-start.4 = (bf16[64,2048]{1,0:T(8,128)(2,1)S(1)}, bf16[64,2048]{1,0:T(8,128)(2,1)}, u32[]{:S(2)}) copy-start(bf16[64,2048]{1,0:T(8,128)(2,1)} %param.19) | copy-start | bytes 786436
  94.1 64.4 %copy-start.7 = (f32[2048]{0:T(1024)S(1)}, f32[2048]{0:T(1024)}, u32[]{:S(2)}) copy-start(f32[2048]{0:T(1024)} %param.31) | copy-start | bytes 24580
  95.6 81.6 %all-gather.7.cloned.1.call-start = ((), (), s32[]{:S(2)}) async-start(), calls=%async_computation.4 | async-start | bytes 1310720 | tf_op jit(solution)/shard_map/all_gather | solution.py:202
  160.3 143.7 %all-gather.11.cloned.1.call-start = ((), (), s32[]{:S(2)}) async-start(), calls=%async_computation.6 | async-start | bytes 9437184 | tf_op jit(solution)/shard_map/all_gather | solution.py:82
  160.9 267.8 %all-gather.9.cloned.1.call-start = ((), (), s32[]{:S(2)}) async-start(), calls=%async_computation.5 | async-start | bytes 9437184 | tf_op jit(solution)/shard_map/all_gather | solution.py:81
  161.5 301.9 %copy-start.5 = (bf16[64,2048]{1,0:T(8,128)(2,1)S(1)}, bf16[64,2048]{1,0:T(8,128)(2,1)}, u32[]{:S(2)}) copy-start(bf16[64,2048]{1,0:T(8,128)(2,1)} %reduce-scatter.3.cloned.1.call-done) | copy-start | bytes 786436
  161.5 301.9 %reduce-scatter.5.cloned.1.call-start = ((), (), s32[]{:S(2)}) async-start(), calls=%async_computation.7 | async-start | bytes 1310720 | tf_op jit(solution)/shard_map/reduce_scatter | solution.py:207
Sparse Core Ops, SparseCore 0:
  9.7 52.0 all-gather.4
  95.7 61.5 reduce-scatter.2
  160.5 16.6 all-gather.6
  179.1 124.9 all-gather.10
  306.0 122.6 all-gather.8
  440.4 22.9 reduce-scatter.4
where the time goes:
time: 474 us; the launch traced here: 472 us
  waiting for transfers between devices  367 us (77%)
  blocking collectives  32.9 us (7%)
  matrix products  26.3 us (6%)
  other arithmetic  13.9 us (3%)
  between operations  13.7 us (3%)
  local copies, waits for them, and re-layouts  12.6 us (3%)
  loops' own time  5.7 us (1%)
    all_gather x1, waiting for transfers between devices, fetch_weights(): lax.all_gather(w_down, 'sp', axis=1, tiled=True)  127 us
    all_gather x1, waiting for transfers between devices, fetch_weights(): lax.all_gather(w_up, 'sp', axis=0, tiled=True)  125 us
    reduce_scatter x1, waiting for transfers between devices, on_device(): lax.psum_scatter((jnp.dot(attn_small, w_out_small, preferred_element_type...  61.7 us
    all_gather x1, blocking collectives, on_device(): lax.all_gather(key_rotated, 'sp', axis=0, tiled=True)  32.9 us
    reduce_scatter x1, waiting for transfers between devices, on_device(): lax.psum_scatter(jnp.dot(hidden, down_full, preferred_element_type=jnp.fl...  23.1 us
    all_gather x1, waiting for transfers between devices, on_device(): lax.all_gather(ffn_normed, 'tp', axis=0, tiled=True)  15.6 us
    all_gather x1, waiting for transfers between devices, on_device(): lax.all_gather(key_normed, 'sp', axis=0, tiled=True)  13.7 us
    dot_general x1, matrix products, on_device(): jnp.dot(hidden, down_full, preferred_element_type=jnp.float32)  11.5 us
  transfers between devices with their start and end apart: 6, of which 6 were waited for; matrix products, arithmetic and copies ran while one was open for 1% of the time, Pallas kernels for 0%

commit v1 on v0

--- a/solution.py
+++ b/solution.py
@@ -1,8 +1,11 @@
+import functools
 import math
 
 import jax
 import jax.numpy as jnp
 from jax import lax
+from jax.experimental import pallas as pl
+from jax.experimental.pallas import tpu as pltpu
 from jax.sharding import PartitionSpec as P
 
 SMALL_DIM = 64
@@ -76,14 +79,317 @@
     return (new_max, row_sum, weighted)
 
 
-def fetch_weights(w_up, w_down):
-    return (
-        lax.all_gather(w_up, "sp", axis=0, tiled=True),
-        lax.all_gather(w_down, "sp", axis=1, tiled=True),
-    )
+MESH = pl.DeviceIdType.MESH
+CORES = 2
+LANES = 128
+
+
+def inner_split(count):
+    best = 1
+    for size in range(1, count + 1):
+        if size * size <= count and count % size == 0:
+            best = size
+    return best
+
+
+def remote(src, dst, send_sem, recv_sem, device):
+    return pltpu.make_async_remote_copy(
+        src_ref=src,
+        dst_ref=dst,
+        send_sem=send_sem,
+        recv_sem=recv_sem,
+        device_id=device,
+        device_id_type=MESH,
+    )
+
+
+def place(ny, nz, nx):
+    s, t = lax.axis_index("sp"), lax.axis_index("tp")
+    z, y = s // ny, s % ny
+    x, c = t // CORES, t % CORES
+
+    def at(zz, yy, xx, cc):
+        return (zz * ny + yy, xx * CORES + cc)
+
+    return z, y, x, c, at
+
+
+def greet(devices):
+    barrier = pltpu.get_barrier_semaphore()
+    for device in devices:
+        pl.semaphore_signal(barrier, inc=1, device_id=device, device_id_type=MESH)
+    pl.semaphore_wait(barrier, len(devices))
+
+
+def spread_kernel(
+    ny, nz, nx, lat_ref, up_ref, dn_ref, lat_out, up_out, dn_out,
+    own_sem, lz_s, lz_r, ly_s, ly_r, lc_s, lc_r, uz_s, uz_r, uy_s, uy_r, dz_s, dz_r, dy_s, dy_r,
+):
+    z, y, x, c, at = place(ny, nz, nx)
+    s = z * ny + y
+    rows = lat_ref.shape[0]
+    half = rows // CORES
+    units = up_out.shape[2]
+    mine = pl.ds(pl.multiple_of(c * half, half), half)
+    other = pl.ds(pl.multiple_of((1 - c) * half, half), half)
+    partner = at(z, y, x, 1 - c)
+    zdev = [at((z + k) % nz, y, x, c) for k in range(nz)]
+    ydev = [at(z, (y + j) % ny, x, c) for j in range(ny)]
+    greet(zdev[1:] + ydev[1:] + [partner])
+
+    def block(k, j):
+        return ((z - k + nz) % nz) * ny + (y - j + ny) % ny
+
+    def up_part(to):
+        return up_ref.at[:, pl.ds(pl.multiple_of(to * units, LANES), units)]
+
+    def dn_part(to):
+        return dn_ref.at[pl.ds(pl.multiple_of(to * units, LANES), units), :]
+
+    sent = []
+
+    def start(*args):
+        copy = remote(*args)
+        copy.start()
+        sent.append(copy)
+
+    for k in range(1, nz):
+        start(lat_ref.at[mine], lat_out.at[s, mine], lz_s.at[k], lz_r.at[k], zdev[k])
+    for j in range(1, ny):
+        start(lat_ref.at[mine], lat_out.at[s, mine], ly_s.at[0, j], ly_r.at[0, j], ydev[j])
+    for k in range(1, nz):
+        to = (z + k) % nz
+        start(up_part(to), up_out.at[s], uz_s.at[k], uz_r.at[k], zdev[k])
+        start(dn_part(to), dn_out.at[s], dz_s.at[k], dz_r.at[k], zdev[k])
+    own = [
+        pltpu.make_async_copy(lat_ref, lat_out.at[s], own_sem.at[0]),
+        pltpu.make_async_copy(up_part(z), up_out.at[s], own_sem.at[1]),
+        pltpu.make_async_copy(dn_part(z), dn_out.at[s], own_sem.at[2]),
+    ]
+    for copy in own:
+        copy.start()
+
+    def to_partner(k, j):
+        slot = lat_out.at[block(k, j), mine]
+        start(slot, slot, lc_s.at[k, j], lc_r.at[k, j], partner)
+
+    for k in range(1, nz):
+        slot = lat_out.at[block(k, 0), mine]
+        remote(slot, slot, lz_s.at[k], lz_r.at[k], zdev[k]).wait_recv()
+        for j in range(1, ny):
+            start(slot, slot, ly_s.at[k, j], ly_r.at[k, j], ydev[j])
+        to_partner(k, 0)
+    for j in range(1, ny):
+        start(up_part(z), up_out.at[s], uy_s.at[0, j], uy_r.at[0, j], ydev[j])
+        start(dn_part(z), dn_out.at[s], dy_s.at[0, j], dy_r.at[0, j], ydev[j])
+    for k in range(nz):
+        for j in range(1, ny):
+            slot = lat_out.at[block(k, j), mine]
+            remote(slot, slot, ly_s.at[k, j], ly_r.at[k, j], ydev[j]).wait_recv()
+            to_partner(k, j)
+    for k in range(nz):
+        for j in range(ny):
+            if k or j:
+                slot = lat_out.at[block(k, j), other]
+                remote(slot, slot, lc_s.at[k, j], lc_r.at[k, j], partner).wait_recv()
+    for copy in own:
+        copy.wait()
+    for k in range(1, nz):
+        for out, ss, rs, sy, ry in (
+            (up_out, uz_s, uz_r, uy_s, uy_r),
+            (dn_out, dz_s, dz_r, dy_s, dy_r),
+        ):
+            slot = out.at[block(k, 0)]
+            remote(slot, slot, ss.at[k], rs.at[k], zdev[k]).wait_recv()
+            for j in range(1, ny):
+                start(slot, slot, sy.at[k, j], ry.at[k, j], ydev[j])
+    for k in range(nz):
+        for j in range(1, ny):
+            for out, sy, ry in ((up_out, uy_s, uy_r), (dn_out, dy_s, dy_r)):
+                slot = out.at[block(k, j)]
+                remote(slot, slot, sy.at[k, j], ry.at[k, j], ydev[j]).wait_recv()
+    for copy in sent:
+        copy.wait_send()
+
+
+def spread(ny, nz, nx, latents, w_up, w_down):
+    rows, width = latents.shape
+    units = w_up.shape[1] // nz
+    sp = ny * nz
+    dma = pltpu.SemaphoreType.DMA
+    vmem = pl.BlockSpec(memory_space=pltpu.VMEM)
+    return pl.pallas_call(
+        functools.partial(spread_kernel, ny, nz, nx),
+        out_shape=(
+            jax.ShapeDtypeStruct((sp, rows, width), latents.dtype),
+            jax.ShapeDtypeStruct((sp, w_up.shape[0], units), w_up.dtype),
+            jax.ShapeDtypeStruct((sp, units, w_down.shape[1]), w_down.dtype),
+        ),
+        in_specs=[vmem] * 3,
+        out_specs=(vmem,) * 3,
+        scratch_shapes=[dma((3,)), dma((nz,)), dma((nz,))]
+        + [dma((nz, ny))] * 4
+        + [dma((nz,)), dma((nz,)), dma((nz, ny)), dma((nz, ny))] * 2,
+        compiler_params=pltpu.CompilerParams(
+            collective_id=1, has_side_effects=True, vmem_limit_bytes=60 * 2**20
+        ),
+        name="spread",
+    )(latents, w_up, w_down)
+
+
+def mixer_kernel(
+    ny, nz, nx, part_ref, resid_ref, gain_ref, up_ref, dn_ref, out_ref,
+    rs_in, after, xg, pbuf, cbuf, xbuf, zsend, zbuf,
+    a_s, a_r, bz_s, bz_r, bx_s, bx_r, bc_s, bc_r, cc_s, cc_r, cx_s, cx_r, cz_s, cz_r,
+):
+    z, y, x, c, at = place(ny, nz, nx)
+    tp = nx * CORES
+    t = x * CORES + c
+    rows, width = resid_ref.shape
+    partner = at(z, y, x, 1 - c)
+    zdev = [at((z + k) % nz, y, x, c) for k in range(nz)]
+    zback = [at((z - k + nz) % nz, y, x, c) for k in range(nz)]
+    xdev = [at(z, y, (x + j) % nx, c) for j in range(nx)]
+    tdev = [(z * ny + y, (t + k) % tp) for k in range(tp)]
+    greet(tdev[1:] + zdev[1:])
+    sent = []
+
+    def start(*args):
+        copy = remote(*args)
+        copy.start()
+        sent.append(copy)
+
+    for k in range(1, tp):
+        start(part_ref.at[(t + k) % tp], rs_in.at[k], a_s.at[k], a_r.at[k], tdev[k])
+    total = resid_ref[...].astype(jnp.float32)
+    mixed = part_ref[t].astype(jnp.float32)
+    for k in range(1, tp):
+        remote(rs_in.at[k], rs_in.at[k], a_s.at[k], a_r.at[k], tdev[k]).wait_recv()
+        mixed = mixed + rs_in[k].astype(jnp.float32)
+    total = (total + mixed).astype(jnp.bfloat16)
+    after[...] = total
+    xg[z, c, x] = rms_scale(total, gain_ref[...]).astype(jnp.bfloat16)
+
+    def zi(k):
+        return (z - k + nz) % nz
+
+    def xi(j):
+        return (x - j + nx) % nx
+
+    def gather_step(k):
+        slot = xg.at[zi(k), c, x]
+        if k == 0:
+            for kk in range(1, nz):
+                start(slot, slot, bz_s.at[kk], bz_r.at[kk], zdev[kk])
+        else:
+            remote(slot, slot, bz_s.at[k], bz_r.at[k], zdev[k]).wait_recv()
+        for j in range(1, nx):
+            start(slot, slot, bx_s.at[k, j], bx_r.at[k, j], xdev[j])
+        start(slot, slot, bc_s.at[k, 0], bc_r.at[k, 0], partner)
+
+    def cross_step(k):
+        for j in range(1, nx):
+            slot = xg.at[zi(k), c, xi(j)]
+            remote(slot, slot, bx_s.at[k, j], bx_r.at[k, j], xdev[j]).wait_recv()
+            start(slot, slot, bc_s.at[k, j], bc_r.at[k, j], partner)
+        for j in range(nx):
+            slot = xg.at[zi(k), 1 - c, xi(j)]
+            remote(slot, slot, bc_s.at[k, j], bc_r.at[k, j], partner).wait_recv()
+
+    def compute_step(k):
+        tokens = xg[zi(k)].reshape(tp * rows, width)
+        projected = jnp.dot(tokens, up_ref[...], preferred_element_type=jnp.float32)
+        hidden = jnp.square(jnp.maximum(projected, 0.0)).astype(jnp.bfloat16)
+        cols = dn_ref.shape[2]
+        for b in range(dn_ref.shape[0]):
+            block = jnp.dot(hidden, dn_ref[b], preferred_element_type=jnp.float32)
+            pbuf[k, :, :, :, b * cols : (b + 1) * cols] = block.astype(jnp.bfloat16).reshape(
+                CORES, nx, rows, cols
+            )
+        start(pbuf.at[k, 1 - c], cbuf.at[k], cc_s.at[k], cc_r.at[k], partner)
+
+    def core_sum(k):
+        remote(cbuf.at[k], cbuf.at[k], cc_s.at[k], cc_r.at[k], partner).wait_recv()
+        pbuf[k, c] = (
+            pbuf[k, c].astype(jnp.float32) + cbuf[k].astype(jnp.float32)
+        ).astype(jnp.bfloat16)
+        for j in range(1, nx):
+            start(pbuf.at[k, c, (x + j) % nx], xbuf.at[k, j], cx_s.at[k, j], cx_r.at[k, j], xdev[j])
+
+    def cross_sum(k):
+        summed = pbuf[k, c, x].astype(jnp.float32)
+        for j in range(1, nx):
+            remote(xbuf.at[k, j], xbuf.at[k, j], cx_s.at[k, j], cx_r.at[k, j], xdev[j]).wait_recv()
+            summed = summed + xbuf[k, j].astype(jnp.float32)
+        zsend[k] = summed.astype(jnp.bfloat16)
+        if k:
+            start(zsend.at[k], zbuf.at[k], cz_s.at[k], cz_r.at[k], zback[k])
+
+    gather_step(0)
+    for k in range(nz):
+        if k + 1 < nz:
+            gather_step(k + 1)
+        cross_step(k)
+        compute_step(k)
+        if k >= 1:
+            core_sum(k - 1)
+        if k >= 2:
+            cross_sum(k - 2)
+    core_sum(nz - 1)
+    for k in range(max(nz - 2, 0), nz):
+        cross_sum(k)
+    final = after[...].astype(jnp.float32)
+    ffn = zsend[0].astype(jnp.float32)
+    for k in range(1, nz):
+        remote(zbuf.at[k], zbuf.at[k], cz_s.at[k], cz_r.at[k], zback[k]).wait_recv()
+        ffn = ffn + zbuf[k].astype(jnp.float32)
+    out_ref[...] = (final + ffn).astype(jnp.bfloat16)
+    for copy in sent:
+        copy.wait_send()
+
+
+def mixer(ny, nz, nx, part, resid, gain, up, dn):
+    tp, rows, width = part.shape
+    dma = pltpu.SemaphoreType.DMA
+    vmem = pl.BlockSpec(memory_space=pltpu.VMEM)
+    b16 = jnp.bfloat16
+
+    def pair(*shape):
+        return [dma(shape), dma(shape)]
+
+    return pl.pallas_call(
+        functools.partial(mixer_kernel, ny, nz, nx),
+        out_shape=jax.ShapeDtypeStruct((rows, width), b16),
+        in_specs=[vmem] * 5,
+        out_specs=vmem,
+        scratch_shapes=[
+            pltpu.VMEM((tp, rows, width), b16),
+            pltpu.VMEM((rows, width), b16),
+            pltpu.VMEM((nz, CORES, nx, rows, width), b16),
+            pltpu.VMEM((nz, CORES, nx, rows, width), b16),
+            pltpu.VMEM((nz, nx, rows, width), b16),
+            pltpu.VMEM((nz, nx, rows, width), b16),
+            pltpu.VMEM((nz, rows, width), b16),
+            pltpu.VMEM((nz, rows, width), b16),
+        ]
+        + pair(tp)
+        + pair(nz)
+        + pair(nz, nx)
+        + pair(nz, nx)
+        + pair(nz)
+        + pair(nz, nx)
+        + pair(nz),
+        compiler_params=pltpu.CompilerParams(
+            collective_id=2, has_side_effects=True, vmem_limit_bytes=60 * 2**20
+        ),
+        name="mixer",
+    )(part, resid, gain, up, dn)
 
 
 def on_device(
+    ny,
+    nz,
+    nx,
     resid,
     q_latent,
     kv_latent,
@@ -132,10 +438,13 @@
         return (small_kv, large_kv, rot_block)
 
     folded = initial
-    pieces = (
-        lax.all_gather(key_normed, "sp", axis=0, tiled=True),
-        lax.all_gather(key_rotated, "sp", axis=0, tiled=True),
-    )
+    rope_pad = jnp.pad(key_rotated, ((0, 0), (0, LANES - ROPE_DIM)))
+    latents, up_mine, down_mine = spread(
+        ny, nz, nx, jnp.concatenate([key_normed, rope_pad], axis=1), w_up, w_down
+    )
+    latents = latents.reshape(-1, latents.shape[-1])
+    rank = key_normed.shape[1]
+    pieces = (latents[:, :rank], latents[:, rank : rank + ROPE_DIM])
     piece_rows = pieces[0].shape[0]
     block_rows = math.gcd(piece_rows, 512)
     block_count = piece_rows // block_rows
@@ -186,36 +495,29 @@
 
     attn_small = finish(folded[0])
     attn_large = finish(folded[1])
-    mixed_rows = lax.psum_scatter(
-        (
-            jnp.dot(attn_small, w_out_small, preferred_element_type=jnp.float32)
-            + jnp.dot(attn_large, w_out_large, preferred_element_type=jnp.float32)
-        ).astype(jnp.bfloat16),
-        "tp",
-        scatter_dimension=0,
-        tiled=True,
-    ).astype(jnp.float32)
-    after_attn = (resid.astype(jnp.float32) + mixed_rows).astype(jnp.bfloat16)
-    ffn_normed = rms_scale(after_attn, ffn_gain).astype(jnp.bfloat16)
-    up_full, down_full = fetch_weights(w_up, w_down)
-    projected = jnp.dot(
-        lax.all_gather(ffn_normed, "tp", axis=0, tiled=True),
-        up_full,
-        preferred_element_type=jnp.float32,
-    )
-    hidden = jnp.square(jax.nn.relu(projected)).astype(jnp.bfloat16)
-    ffn_rows = lax.psum_scatter(
-        jnp.dot(hidden, down_full, preferred_element_type=jnp.float32).astype(jnp.bfloat16),
-        "tp",
-        scatter_dimension=0,
-        tiled=True,
-    ).astype(jnp.float32)
-    return (after_attn.astype(jnp.float32) + ffn_rows).astype(jnp.bfloat16)
+    part = (
+        jnp.dot(attn_small, w_out_small, preferred_element_type=jnp.float32)
+        + jnp.dot(attn_large, w_out_large, preferred_element_type=jnp.float32)
+    ).astype(jnp.bfloat16)
+    width = part.shape[1]
+    return mixer(
+        ny,
+        nz,
+        nx,
+        part.reshape(nx * CORES, -1, width),
+        resid,
+        ffn_gain.reshape(1, width),
+        up_mine.reshape(width, -1),
+        down_mine,
+    )
 
 
 def solution(mesh):
+    ny = inner_split(mesh.shape["sp"])
+    nz = mesh.shape["sp"] // ny
+    nx = mesh.shape["tp"] // CORES
     return jax.shard_map(
-        on_device,
+        functools.partial(on_device, ny, nz, nx),
         mesh=mesh,
         in_specs=(
             P(("sp", "tp"), None),

time: 474 us -> 255 us (0.54)
  waiting for transfers between devices: 367 us -> 0 us
  Pallas kernels: 0 us -> 209 us
  blocking collectives: 32.9 us -> 0 us
  matrix products: 26.3 us -> 12.2 us
  between operations: 13.7 us -> 0.19 us
  local copies, waits for them, and re-layouts: 12.6 us -> 19.4 us
  other arithmetic: 13.9 us -> 7.55 us
    all_gather x4 -> x0, waiting for transfers between devices: 281 us -> none  [the longest x1 127 us: fetch_weights(): lax.all_gather(w_down, 'sp', axis=1, tiled=True)]
    pallas_call x0 -> x2, Pallas kernels: none -> 209 us  [the longest x1 131 us: mixer(): pl.pallas_call(functools.partial(mixer_kernel, ny, nz, nx), out_shape=jax...]
    reduce_scatter x2 -> x0, waiting for transfers between devices: 84.8 us -> none  [the longest x1 61.7 us: on_device(): lax.psum_scatter((jnp.dot(attn_small, w_out_small, preferred_element_type...]
    all_gather x1 -> x0, blocking collectives: 32.9 us -> none  [on_device(): lax.all_gather(key_rotated, 'sp', axis=0, tiled=True)]
    dot_general x1 -> x0, matrix products: 11.5 us -> none  [on_device(): jnp.dot(hidden, down_full, preferred_element_type=jnp.float32)]
  transfers between devices with their start and end apart: 6 -> 0, of which waited for: 6 -> 0; matrix products, arithmetic and copies ran while one was open for 1% -> 0% of each run, Pallas kernels for 0% -> 0%
where the time goes in v1:
time: 255 us; the launch traced here: 254 us
  Pallas kernels  209 us (82%)
  local copies, waits for them, and re-layouts  19.4 us (8%)
  matrix products  12.2 us (5%)
  other arithmetic  7.55 us (3%)
  loops' own time  5.22 us (2%)
    pallas_call x1, Pallas kernels, mixer(): pl.pallas_call(functools.partial(mixer_kernel, ny, nz, nx), out_shape=jax...  131 us
    pallas_call x1, Pallas kernels, spread(): pl.pallas_call(functools.partial(spread_kernel, ny, nz, nx), out_shape=(j...  78 us

profile of v1, /device:TPU:0, one launch (start us, length us, event | category | flops | bytes accessed | tf_op | source)
XLA Modules:
  0.0 253.7 jit_solution(16355019088564750143)
XLA Ops:
  0.1 0.5 iota.18
  0.5 1.1 fusion.47
  1.7 1.2 fusion.43
  2.9 0.7 convert_element_type.75
  3.6 0.1 multiply_cosine_fusion
  3.7 0.1 copy.68
  3.9 1.5 fusion.53
  5.4 0.1 fusion.49
  5.5 0.8 fusion.50.lat_ref
  6.3 0.4 fusion.51
  6.8 0.6 pad_maximum_fusion.1
  7.4 0.1 copy.71
  7.5 78.0 %spread.1 = (bf16[8,256,640]{2,1,0:T(8,128)(2,1)}, bf16[8,256,512]{2,1,0:T(8,128)(2,1)}, bf16[8,512,256]{2,1,0:T(8,128)(2,1)}) custom-call(bf16[256,640]{1,0:T(8,128)(2,1)} %fusion.50.lat_ref, bf16[256,2048]{1,0:T(8,128)(2,1)} %up_ref.1, bf16[2048,256]{1,0:T(8,128)(2,1)} %dn_ref.1), custom_call_target="tpu_custom_call" | custom-call | tf_op jit(solution)/shard_map/spread/pallas_call | solution.py:221
  85.6 1.9 slice.103
  87.4 1.7 slice.99
  89.2 1.9 copy.70
  91.1 0.6 broadcast.131
  91.6 0.7 broadcast_in_dim.65
  92.3 0.7 broadcast_in_dim.66
  93.0 22.9 %while.21 = (s32[]{:T(128)}, f32[2,256]{1,0:T(2,128)S(1)}, f32[2,256]{1,0:T(2,128)}, f32[2,256,64]{1,2,0:T(8,128)}, f32[2,256]{1,0:T(2,128)S(1)}, /*index=5*/f32...) while((s32[]{:T(128)}, f32[2,256]{1,0:T(2,128)S(1)}, ...), condition=%wide.region_9.10_spmd.clone, body=%wide.region_2.9_spmd.clone.sunk | while | flops 643500800 | bytes 19211336 | solution.py:489
  93.0 1.2 dynamic_slice.44
  94.8 0.5 slice.144
  96.0 10.9 %conditional.3 = ((f32[2,256]{1,0:T(2,128)S(1)}, f32[2,256]{1,0:T(2,128)}, f32[2,256,64]{1,2,0:T(8,128)}, f32[2,256]{1,0:T(2,128)S(1)}, f32[2,256]{1,0:T(2,128)S(1)}, /*index=5*/f32[2,256,128]{2,1,0:T(8,128)})) conditional(s32[]{:T(128)} %convert_element_type.120, (f32[2,256]{1,0:T(2,128)S(1)}, f32[2,256]{1,0:T(2,128)}, f32[2,256,64]{1,2,0:T(8,128)}, ...), branch_computations={%region_3.3_spmd, %region_4.8_spmd} | conditional | flops 643500288 | bytes 19207864 | solution.py:486
  96.0 0.1 broadcast_compare_fusion
  96.2 0.8 copy.65
  97.0 1.3 convolution_convert_fusion.1
  98.3 1.5 convolution_convert_fusion
  99.8 0.3 convolution_bitcast_fusion
  100.2 1.1 fusion.56
  101.4 0.3 convolution_bitcast_fusion.3
  101.7 0.4 fusion.55
  102.1 0.4 fusion.11
  102.5 1.3 multiply_add_fusion
  103.8 1.9 convolution_add_fusion.1
  105.6 0.5 convolution_add_fusion
  106.2 0.7 copy-done.2
  106.9 1.2 dynamic_slice.44
  108.7 0.5 slice.144
  109.9 1.2 dynamic_slice.44
  111.7 0.5 slice.144
  112.9 1.2 dynamic_slice.44
  114.7 0.5 slice.144
  115.9 1.1 copy.72
  117.0 0.9 divide_convert_fusion.1
  118.0 1.5 fusion.57
  119.5 1.4 fusion.42
  120.9 131.2 %mixer.1 = bf16[64,2048]{1,0:T(8,128)(2,1)} custom-call(bf16[4,64,2048]{2,1,0:T(8,128)(2,1)} %bitcast.70, bf16[64,2048]{1,0:T(8,128)(2,1)} %resid_ref.1, f32[1,2048]{1,0:T(1,128)} %bitcast.81, bf16[2048,512]{1,0:T(8,128)(2,1)} %bitcast.74, bf16[8,512,256]{2,1,0:T(8,128)(2,1)} %get-tuple-element.233.dn_ref), custom_call_target="tpu_custom_call" | custom-call | tf_op jit(solution)/shard_map/mixer/pallas_call | solution.py:360
  252.1 1.7 copy.116
  (48 shorter events, 0.3 us)
Async XLA Ops:
  0.0 119.5 %copy-start = (bf16[256,2048]{1,0:T(8,128)(2,1)S(1)}, bf16[256,2048]{1,0:T(8,128)(2,1)}, u32[]{:S(2)}) copy-start(bf16[256,2048]{1,0:T(8,128)(2,1)} %param.30) | copy-start | bytes 3145732
  0.0 6.3 %copy-start.6 = (bf16[256,768]{1,0:T(8,128)(2,1)S(1)}, bf16[256,768]{1,0:T(8,128)(2,1)}, u32[]{:S(2)}) copy-start(bf16[256,768]{1,0:T(8,128)(2,1)} %param.20) | copy-start | bytes 1179652
  0.0 6.3 %copy-start.9 = (f32[768]{0:T(1024)S(1)}, f32[768]{0:T(1024)}, u32[]{:S(2)}) copy-start(f32[768]{0:T(1024)} %param.23) | copy-start | bytes 9220
  0.0 5.3 %copy-start.5 = (bf16[256,512]{1,0:T(8,128)(2,1)S(1)}, bf16[256,512]{1,0:T(8,128)(2,1)}, u32[]{:S(2)}) copy-start(bf16[256,512]{1,0:T(8,128)(2,1)} %param.21) | copy-start | bytes 786436
  0.0 6.3 %copy-start.8 = (bf16[768,320]{0,1:T(8,128)(2,1)S(1)}, bf16[768,320]{0,1:T(8,128)(2,1)}, u32[]{:S(2)}) copy-start(bf16[768,320]{0,1:T(8,128)(2,1)} %param.26) | copy-start | bytes 1474564
  0.0 5.3 %copy-start.7 = (f32[512]{0:T(512)S(1)}, f32[512]{0:T(512)}, u32[]{:S(2)}) copy-start(f32[512]{0:T(512)} %param.24) | copy-start | bytes 6148
  97.0 3.2 %copy-start.4 = (bf16[4,512,32]{1,2,0:T(8,128)(2,1)S(1)}, bf16[4,512,32]{1,2,0:T(8,128)(2,1)}, u32[]{:S(2)}) copy-start(bf16[4,512,32]{1,2,0:T(8,128)(2,1)} %get-tuple-element.189) | copy-start | bytes 393220 | tf_op jit(solution)/shard_map/while/body/eval_jaxpr/cond
  99.8 1.5 copy-start.3
  102.1 3.5 %copy-start.1 = (f32[2,256,128]{2,1,0:T(8,128)S(1)}, f32[2,256,128]{2,1,0:T(8,128)}, u32[]{:S(2)}) copy-start(f32[2,256,128]{2,1,0:T(8,128)} %get-tuple-element.196) | copy-start | bytes 786436 | tf_op jit(solution)/shard_map/while/body/eval_jaxpr/cond
  106.1 0.7 copy-start.2

commit v2 on v1

v2 whole, which is shorter than its diff:
```python
import functools

import jax
import jax.numpy as jnp
from jax import lax
from jax.experimental import pallas as pl
from jax.experimental.pallas import tpu as pltpu
from jax.sharding import PartitionSpec as P

SMALL_DIM = 64
LARGE_DIM = 128
ROPE_DIM = 32


epsilon = 1e-06
theta_base = 10000.0
mask_floor = -1e30


def rms_scale(inputs, gain_vec):
    values = inputs.astype(jnp.float32)
    return (
        values * lax.rsqrt(jnp.mean(values * values, axis=-1, keepdims=True) + epsilon) * gain_vec
    )


def rotary(values, positions):
    halfway = values.shape[-1] // 2
    inverse = theta_base ** (-jnp.arange(0, 2 * halfway, 2, dtype=jnp.float32) / (2 * halfway))
    angles = positions.astype(jnp.float32)[:, None] * inverse[None, :]
    cos_table = jnp.cos(angles)
    sin_table = jnp.sin(angles)
    if values.ndim == 3:
        cos_table = cos_table[:, None, :]
        sin_table = sin_table[:, None, :]
    first_half = values[..., :halfway]
    second_half = values[..., halfway:]
    return jnp.concatenate(
        [
            first_half * cos_table - second_half * sin_table,
            second_half * cos_table + first_half * sin_table,
        ],
        axis=-1,
    )


def queries(normed, weight, nope_dim, positions):
    projected = jnp.dot(normed, weight, preferred_element_type=jnp.float32)
    projected = projected.reshape(projected.shape[0], -1, nope_dim + ROPE_DIM)
    turned = rotary(projected[..., nope_dim:], positions)
    return jnp.concatenate([projected[..., :nope_dim], turned], axis=-1).astype(jnp.bfloat16)


MESH = pl.DeviceIdType.MESH
CORES = 2
LANES = 128


def inner_split(count):
    best = 1
    for size in range(1, count + 1):
        if size * size <= count and count % size == 0:
            best = size
    return best


def remote(src, dst, send_sem, recv_sem, device):
    return pltpu.make_async_remote_copy(
        src_ref=src,
        dst_ref=dst,
        send_sem=send_sem,
        recv_sem=recv_sem,
        device_id=device,
        device_id_type=MESH,
    )


def place(ny, nz, nx):
    s, t = lax.axis_index("sp"), lax.axis_index("tp")
    z, y = s // ny, s % ny
    x, c = t // CORES, t % CORES

    def at(zz, yy, xx, cc):
        return (zz * ny + yy, xx * CORES + cc)

    return z, y, x, c, at


def greet(devices):
    barrier = pltpu.get_barrier_semaphore()
    for device in devices:
        pl.semaphore_signal(barrier, inc=1, device_id=device, device_id_type=MESH)
    pl.semaphore_wait(barrier, len(devices))


def layer_kernel(
    ny, nz, nx, lat_ref, q_ref, wks_ref, wkl_ref, wos_ref, wol_ref, resid_ref, gain_ref, up_ref,
    dn_ref, out_ref, lat_out, up_out, dn_out, row_max, row_sum, weighted, part_ref,
    rs_in, after, xg, pbuf, cbuf, xbuf, zsend, zbuf, own_sem,
    lz_s, lz_r, ly_s, ly_r, lc_s, lc_r, uz_s, uz_r, uy_s, uy_r, dz_s, dz_r, dy_s, dy_r,
    a_s, a_r, bz_s, bz_r, bx_s, bx_r, bc_s, bc_r, cc_s, cc_r, cx_s, cx_r, cz_s, cz_r,
):
    z, y, x, c, at = place(ny, nz, nx)
    s = z * ny + y
    rows = lat_ref.shape[0]
    half = rows // CORES
    units = up_out.shape[2]
    tp = nx * CORES
    t = x * CORES + c
    mine = pl.ds(pl.multiple_of(c * half, half), half)
    other = pl.ds(pl.multiple_of((1 - c) * half, half), half)
    partner = at(z, y, x, 1 - c)
    zdev = [at((z + k) % nz, y, x, c) for k in range(nz)]
    ydev = [at(z, (y + j) % ny, x, c) for j in range(ny)]
    zback = [at((z - k + nz) % nz, y, x, c) for k in range(nz)]
    xdev = [at(z, y, (x + j) % nx, c) for j in range(nx)]
    tdev = [(s, (t + k) % tp) for k in range(tp)]
    greet(zdev[1:] + ydev[1:] + tdev[1:])

    def block(k, j):
        return ((z - k + nz) % nz) * ny + (y - j + ny) % ny

    def up_part(to):
        return up_ref.at[:, pl.ds(pl.multiple_of(to * units, LANES), units)]

    def dn_part(to):
        return dn_ref.at[pl.ds(pl.multiple_of(to * units, LANES), units), :]

    sent = []

    def start(*args):
        copy = remote(*args)
        copy.start()
        sent.append(copy)

    for k in range(1, nz):
        start(lat_ref.at[mine], lat_out.at[s, mine], lz_s.at[k], lz_r.at[k], zdev[k])
    for j in range(1, ny):
        start(lat_ref.at[mine], lat_out.at[s, mine], ly_s.at[0, j], ly_r.at[0, j], ydev[j])
    for k in range(1, nz):
        to = (z + k) % nz
        start(up_part(to), up_out.at[s], uz_s.at[k], uz_r.at[k], zdev[k])
        start(dn_part(to), dn_out.at[s], dz_s.at[k], dz_r.at[k], zdev[k])
    own = [
        pltpu.make_async_copy(lat_ref, lat_out.at[s], own_sem.at[0]),
        pltpu.make_async_copy(up_part(z), up_out.at[s], own_sem.at[1]),
        pltpu.make_async_copy(dn_part(z), dn_out.at[s], own_sem.at[2]),
    ]
    for copy in own:
        copy.start()

    def to_partner(k, j):
        slot = lat_out.at[block(k, j), mine]
        start(slot, slot, lc_s.at[k, j], lc_r.at[k, j], partner)

    for k in range(1, nz):
        slot = lat_out.at[block(k, 0), mine]
        remote(slot, slot, lz_s.at[k], lz_r.at[k], zdev[k]).wait_recv()
        for j in range(1, ny):
            start(slot, slot, ly_s.at[k, j], ly_r.at[k, j], ydev[j])
        to_partner(k, 0)
    for j in range(1, ny):
        start(up_part(z), up_out.at[s], uy_s.at[0, j], uy_r.at[0, j], ydev[j])
        start(dn_part(z), dn_out.at[s], dy_s.at[0, j], dy_r.at[0, j], ydev[j])
    for k in range(nz):
        for j in range(1, ny):
            slot = lat_out.at[block(k, j), mine]
            remote(slot, slot, ly_s.at[k, j], ly_r.at[k, j], ydev[j]).wait_recv()
            to_partner(k, j)
    for k in range(nz):
        for j in range(ny):
            if k or j:
                slot = lat_out.at[block(k, j), other]
                remote(slot, slot, lc_s.at[k, j], lc_r.at[k, j], partner).wait_recv()
    for copy in own:
        copy.wait()

    def forward(k):
        for out, ss, rs, sy, ry in (
            (up_out, uz_s, uz_r, uy_s, uy_r),
            (dn_out, dz_s, dz_r, dy_s, dy_r),
        ):
            slot = out.at[block(k, 0)]
            remote(slot, slot, ss.at[k], rs.at[k], zdev[k]).wait_recv()
            for j in range(1, ny):
                start(slot, slot, sy.at[k, j], ry.at[k, j], ydev[j])

    rank = wks_ref.shape[0]
    heads = q_ref.shape[0]
    small = wks_ref.shape[1] // (2 * SMALL_DIM)
    row_max[...] = jnp.full_like(row_max, mask_floor)
    row_sum[...] = jnp.zeros_like(row_sum)
    weighted[...] = jnp.zeros_like(weighted)
    ahead = lax.broadcasted_iota(jnp.int32, (rows, rows), 1) - lax.broadcasted_iota(
        jnp.int32, (rows, rows), 0
    )

    def key_step(j, carry):
        latent = lat_out[j, :, :rank]
        turned = lat_out[j, :, rank:]
        kv_small = jnp.dot(latent, wks_ref[...], preferred_element_type=jnp.float32)
        kv_small = kv_small.astype(jnp.bfloat16)
        kv_large = jnp.dot(latent, wkl_ref[...], preferred_element_type=jnp.float32)
        kv_large = kv_large.astype(jnp.bfloat16)
        causal = ahead <= (s - j) * rows
        for h in range(heads):
            if h < small:
                key = kv_small[:, 2 * SMALL_DIM * h : 2 * SMALL_DIM * (h + 1)]
                value = key
                scale = (SMALL_DIM + ROPE_DIM) ** (-0.5)
            else:
                first = 2 * LARGE_DIM * (h - small)
                key = kv_large[:, first : first + LARGE_DIM]
                value = kv_large[:, first + LARGE_DIM : first + 2 * LARGE_DIM]
                scale = (LARGE_DIM + ROPE_DIM) ** (-0.5)
            scores = lax.dot_general(
                q_ref[h],
                jnp.concatenate([key, turned], axis=1),
                (((1,), (1,)), ((), ())),
                preferred_element_type=jnp.float32,
            )
            scores = jnp.where(causal, scores * scale, mask_floor)
            old_max = row_max[h]
            new_max = jnp.maximum(old_max, jnp.max(scores, axis=-1, keepdims=True))
            shrink = jnp.exp(old_max - new_max)
            weights = jnp.exp(scores - new_max)
            row_max[h] = new_max
            row_sum[h] = row_sum[h] * shrink + jnp.sum(weights, axis=-1, keepdims=True)
            weighted[h] = weighted[h] * shrink + jnp.dot(
                weights.astype(jnp.bfloat16), value, preferred_element_type=jnp.float32
            )
        return carry

    middle = (s + 1) // 2
    lax.fori_loop(0, middle, key_step, 0)
    if nz > 1:
        forward(1)
    lax.fori_loop(middle, s + 1, key_step, 0)
    for k in range(2, nz - 1):
        forward(k)
    parts = []
    for h in range(heads):
        head_out = (weighted[h] / row_sum[h]).astype(jnp.bfloat16)
        parts.append(head_out[:, SMALL_DIM:] if h < small else head_out)
    mixed_part = jnp.dot(
        jnp.concatenate(parts[:small], axis=1), wos_ref[...], preferred_element_type=jnp.float32
    ) + jnp.dot(
        jnp.concatenate(parts[small:], axis=1), wol_ref[...], preferred_element_type=jnp.float32
    )
    part_ref[...] = mixed_part.astype(jnp.bfloat16).reshape(part_ref.shape)
    rows, width = resid_ref.shape
    for k in range(1, tp):
        start(part_ref.at[(t + k) % tp], rs_in.at[k], a_s.at[k], a_r.at[k], tdev[k])
    if nz > 2:
        forward(nz - 1)
    total = resid_ref[...].astype(jnp.float32)
    mixed = part_ref[t].astype(jnp.float32)
    for k in range(1, tp):
        remote(rs_in.at[k], rs_in.at[k], a_s.at[k], a_r.at[k], tdev[k]).wait_recv()
        mixed = mixed + rs_in[k].astype(jnp.float32)
    total = (total + mixed).astype(jnp.bfloat16)
    after[...] = total
    xg[z, c, x] = rms_scale(total, gain_ref[...]).astype(jnp.bfloat16)

    def zi(k):
        return (z - k + nz) % nz

    def xi(j):
        return (x - j + nx) % nx

    def gather_step(k):
        slot = xg.at[zi(k), c, x]
        if k == 0:
            for kk in range(1, nz):
                start(slot, slot, bz_s.at[kk], bz_r.at[kk], zdev[kk])
        else:
            remote(slot, slot, bz_s.at[k], bz_r.at[k], zdev[k]).wait_recv()
        for j in range(1, nx):
            start(slot, slot, bx_s.at[k, j], bx_r.at[k, j], xdev[j])
        start(slot, slot, bc_s.at[k, 0], bc_r.at[k, 0], partner)

    def cross_step(k):
        for j in range(1, nx):
            slot = xg.at[zi(k), c, xi(j)]
            remote(slot, slot, bx_s.at[k, j], bx_r.at[k, j], xdev[j]).wait_recv()
            start(slot, slot, bc_s.at[k, j], bc_r.at[k, j], partner)
        for j in range(nx):
            slot = xg.at[zi(k), 1 - c, xi(j)]
            remote(slot, slot, bc_s.at[k, j], bc_r.at[k, j], partner).wait_recv()

    def compute_step(k):
        tokens = xg[zi(k)].reshape(tp * rows, width)
        projected = jnp.dot(tokens, up_out[...].reshape(width, units), preferred_element_type=jnp.float32)
        hidden = jnp.square(jnp.maximum(projected, 0.0)).astype(jnp.bfloat16)
        cols = dn_out.shape[2]
        for b in range(dn_out.shape[0]):
            block = jnp.dot(hidden, dn_out[b], preferred_element_type=jnp.float32)
            pbuf[k, :, :, :, b * cols : (b + 1) * cols] = block.astype(jnp.bfloat16).reshape(
                CORES, nx, rows, cols
            )
        start(pbuf.at[k, 1 - c], cbuf.at[k], cc_s.at[k], cc_r.at[k], partner)

    def core_sum(k):
        remote(cbuf.at[k], cbuf.at[k], cc_s.at[k], cc_r.at[k], partner).wait_recv()
        pbuf[k, c] = (
            pbuf[k, c].astype(jnp.float32) + cbuf[k].astype(jnp.float32)
        ).astype(jnp.bfloat16)
        for j in range(1, nx):
            start(pbuf.at[k, c, (x + j) % nx], xbuf.at[k, j], cx_s.at[k, j], cx_r.at[k, j], xdev[j])

    def cross_sum(k):
        summed = pbuf[k, c, x].astype(jnp.float32)
        for j in range(1, nx):
            remote(xbuf.at[k, j], xbuf.at[k, j], cx_s.at[k, j], cx_r.at[k, j], xdev[j]).wait_recv()
            summed = summed + xbuf[k, j].astype(jnp.float32)
        zsend[k] = summed.astype(jnp.bfloat16)
        if k:
            start(zsend.at[k], zbuf.at[k], cz_s.at[k], cz_r.at[k], zback[k])

    def weights_here():
        for k in range(nz):
            for j in range(1, ny):
                for out, sy, ry in ((up_out, uy_s, uy_r), (dn_out, dy_s, dy_r)):
                    slot = out.at[block(k, j)]
                    remote(slot, slot, sy.at[k, j], ry.at[k, j], ydev[j]).wait_recv()

    gather_step(0)
    for k in range(nz):
        if k + 1 < nz:
            gather_step(k + 1)
        cross_step(k)
        if k == 0:
            weights_here()
        compute_step(k)
        if k >= 1:
            core_sum(k - 1)
        if k >= 2:
            cross_sum(k - 2)
    core_sum(nz - 1)
    for k in range(max(nz - 2, 0), nz):
        cross_sum(k)
    final = after[...].astype(jnp.float32)
    ffn = zsend[0].astype(jnp.float32)
    for k in range(1, nz):
        remote(zbuf.at[k], zbuf.at[k], cz_s.at[k], cz_r.at[k], zback[k]).wait_recv()
        ffn = ffn + zbuf[k].astype(jnp.float32)
    out_ref[...] = (final + ffn).astype(jnp.bfloat16)
    for copy in sent:
        copy.wait_send()


def layer(ny, nz, nx, latents, q_all, wks, wkl, wos, wol, resid, gain, w_up, w_down):
    tp, sp = nx * CORES, ny * nz
    rows, width = resid.shape
    tok_rows = latents.shape[0]
    heads = q_all.shape[0]
    units = w_up.shape[1] // nz
    dma = pltpu.SemaphoreType.DMA
    vmem = pl.BlockSpec(memory_space=pltpu.VMEM)
    b16 = jnp.bfloat16

    def pair(*shape):
        return [dma(shape), dma(shape)]

    return pl.pallas_call(
        functools.partial(layer_kernel, ny, nz, nx),
        out_shape=jax.ShapeDtypeStruct((rows, width), b16),
        in_specs=[vmem] * 10,
        out_specs=vmem,
        scratch_shapes=[
            pltpu.VMEM((sp,) + latents.shape, b16),
            pltpu.VMEM((sp, w_up.shape[0], units), b16),
            pltpu.VMEM((sp, units, w_down.shape[1]), b16),
            pltpu.VMEM((heads, tok_rows, 1), jnp.float32),
            pltpu.VMEM((heads, tok_rows, 1), jnp.float32),
            pltpu.VMEM((heads, tok_rows, LARGE_DIM), jnp.float32),
            pltpu.VMEM((tp, rows, width), b16),
            pltpu.VMEM((tp, rows, width), b16),
            pltpu.VMEM((rows, width), b16),
            pltpu.VMEM((nz, CORES, nx, rows, width), b16),
            pltpu.VMEM((nz, CORES, nx, rows, width), b16),
            pltpu.VMEM((nz, nx, rows, width), b16),
            pltpu.VMEM((nz, nx, rows, width), b16),
            pltpu.VMEM((nz, rows, width), b16),
            pltpu.VMEM((nz, rows, width), b16),
            dma((3,)),
        ]
        + pair(nz)
        + pair(nz, ny) * 2
        + (pair(nz) + pair(nz, ny)) * 2
        + pair(tp)
        + pair(nz)
        + pair(nz, nx)
        + pair(nz, nx)
        + pair(nz)
        + pair(nz, nx)
        + pair(nz),
        compiler_params=pltpu.CompilerParams(
            collective_id=1, has_side_effects=True, vmem_limit_bytes=63 * 2**20
        ),
        name="layer",
    )(latents, q_all, wks, wkl, wos, wol, resid, gain, w_up, w_down)


def on_device(
    ny,
    nz,
    nx,
    resid,
    q_latent,
    kv_latent,
    rope_key,
    q_gain,
    kv_gain,
    w_q_small,
    w_q_large,
    w_kv_small,
    w_kv_large,
    w_out_small,
    w_out_large,
    ffn_gain,
    w_up,
    w_down,
):
    tok_rows = q_latent.shape[0]
    offset = lax.axis_index("sp") * tok_rows
    positions = offset + jnp.arange(tok_rows, dtype=jnp.int32)
    query_normed = rms_scale(q_latent, q_gain).astype(jnp.bfloat16)
    query_small = queries(query_normed, w_q_small, SMALL_DIM, positions)
    query_large = queries(query_normed, w_q_large, LARGE_DIM, positions)
    key_normed = rms_scale(kv_latent, kv_gain).astype(jnp.bfloat16)
    key_rotated = rotary(rope_key.astype(jnp.float32), positions).astype(jnp.bfloat16)
    rope_pad = ((0, 0), (0, LANES - ROPE_DIM))
    latents = jnp.concatenate([key_normed, jnp.pad(key_rotated, rope_pad)], axis=1)

    def head_rows(query, nope_dim):
        content = jnp.pad(query[..., :nope_dim], ((0, 0), (0, 0), (0, LARGE_DIM - nope_dim)))
        turned = jnp.pad(query[..., nope_dim:], ((0, 0),) + rope_pad)
        return jnp.transpose(jnp.concatenate([content, turned], axis=-1), (1, 0, 2))

    q_all = jnp.concatenate(
        [head_rows(query_small, SMALL_DIM), head_rows(query_large, LARGE_DIM)], axis=0
    )
    return layer(
        ny,
        nz,
        nx,
        latents,
        q_all,
        w_kv_small,
        w_kv_large,
        w_out_small,
        w_out_large,
        resid,
        ffn_gain.reshape(1, -1),
        w_up,
        w_down,
    )


def solution(mesh):
    ny = inner_split(mesh.shape["sp"])
    nz = mesh.shape["sp"] // ny
    nx = mesh.shape["tp"] // CORES
    return jax.shard_map(
        functools.partial(on_device, ny, nz, nx),
        mesh=mesh,
        in_specs=(
            P(("sp", "tp"), None),
            P("sp", None),
            P("sp", None),
            P("sp", None),
            P(),
            P(),
            P(None, "tp"),
            P(None, "tp"),
            P(None, "tp"),
            P(None, "tp"),
            P("tp", None),
            P("tp", None),
            P(),
            P("sp", "tp"),
            P("tp", "sp"),
        ),
        out_specs=P(("sp", "tp"), None),
        check_vma=False,
    )
```

time: 255 us -> 154 us (0.60)
  Pallas kernels: 209 us -> 146 us
  local copies, waits for them, and re-layouts: 19.4 us -> 3.54 us
  matrix products: 12.2 us -> 0.77 us
  loops' own time: 5.22 us -> 0 us
  other arithmetic: 7.55 us -> 4.12 us
    pallas_call x2 -> x1, Pallas kernels: 209 us -> 146 us  [layer(): pl.pallas_call(functools.partial(layer_kernel, ny, nz, nx), out_shape=jax...]
    dot_general x10 -> x0, matrix products: 10.3 us -> none  [the longest x2 2.36 us: update_group(): jnp.einsum('hqk,khd->hqd', weights.astype(jnp.bfloat16), value_block, pre...]
    slice x6 -> x0, local copies, waits for them, and re-layouts: 5.78 us -> none  [the longest x2 3.61 us: on_device(): pieces = (latents[:, :rank], latents[:, rank:rank + ROPE_DIM])]
    another operation x5 -> x0, loops' own time: 5.22 us -> none  [the longest x1 5.04 us: on_device(): lax.scan(key_step, folded, (blocked, jnp.arange(block_count, dtype=jnp.in...]
    dynamic_slice x4 -> x0, local copies, waits for them, and re-layouts: 4.74 us -> none  [on_device(): lax.scan(key_step, folded, (blocked, jnp.arange(block_count, dtype=jnp.in...]
where the time goes in v2:
time: 154 us
  Pallas kernels  146 us (95%)
  other arithmetic  4.12 us (3%)
  local copies, waits for them, and re-layouts  3.54 us (2%)
    pallas_call x1, Pallas kernels, layer(): pl.pallas_call(functools.partial(layer_kernel, ny, nz, nx), out_shape=jax...  146 us
    unnamed x15, local copies, waits for them, and re-layouts  3.14 us

profile of v2, /device:TPU:0, one launch (start us, length us, event | category | flops | bytes accessed | tf_op | source)
XLA Modules:
  0.0 154.2 jit_solution(10625501533364850122)
XLA Ops:
  0.0 0.0 copy-start
  0.0 0.0 copy-start.2
  0.0 0.8 convert_element_type.36
  0.8 0.1 multiply_cosine_fusion
  1.0 0.0 copy-start.5
  1.0 1.2 fusion
  2.2 0.0 copy-done
  2.2 0.0 copy-done.2
  2.2 0.0 copy-done.5
  2.2 0.0 copy-start.4
  2.2 0.4 fusion.15
  2.6 0.5 copy-done.4
  3.2 0.4 fusion.17
  3.6 0.1 copy.31
  3.7 0.1 copy.34
  3.9 0.1 copy.33
  4.0 0.1 copy.35
  4.2 0.1 fusion.14
  4.2 0.0 copy-start.1
  4.2 0.8 pad_maximum_fusion.q_ref
  5.1 0.1 copy.29
  5.2 0.0 copy-done.1
  5.2 0.1 fusion.4
  5.3 0.0 copy-start.3
  5.4 0.7 copy-done.3
  6.0 0.1 fusion.6
  6.2 0.8 fusion.10.lat_ref
  6.9 145.6 %layer.1 = bf16[64,2048]{1,0:T(8,128)(2,1)} custom-call(bf16[256,640]{1,0:T(8,128)(2,1)} %fusion.10.lat_ref, bf16[4,256,256]{2,1,0:T(8,128)(2,1)} %pad_maximum_fusion.q_ref, bf16[512,256]{1,0:T(8,128)(2,1)} %wks_ref.1, bf16[512,512]{1,0:T(8,128)(2,1)} %wkl_ref.1, bf16[128,2048]{1,0:T(8,128)(2,1)} %wos_ref.1, bf16[256,2048]{1,0:T(8,128)(2,1)} %wol_ref.1, ...), custom_call_target="tpu_custom_call" | custom-call | tf_op jit(solution)/shard_map/layer/pallas_call | solution.py:365
  152.5 1.7 %copy.37 = bf16[64,2048]{1,0:T(8,128)(2,1)} copy(bf16[64,2048]{1,0:T(8,128)(2,1)} %layer.1) | data formatting | bytes 524288
  (10 shorter events, 0.1 us)
Async XLA Ops:
  0.0 2.2 %copy-start = (bf16[768,320]{0,1:T(8,128)(2,1)S(1)}, bf16[768,320]{0,1:T(8,128)(2,1)}, u32[]{:S(2)}) copy-start(bf16[768,320]{0,1:T(8,128)(2,1)} %param.22) | copy-start | bytes 1474564
  0.0 2.2 %copy-start.2 = (bf16[256,768]{1,0:T(8,128)(2,1)S(1)}, bf16[256,768]{1,0:T(8,128)(2,1)}, u32[]{:S(2)}) copy-start(bf16[256,768]{1,0:T(8,128)(2,1)} %param.16) | copy-start | bytes 1179652
  1.0 1.2 copy-start.5
  2.2 1.0 copy-start.4
  4.2 1.0 copy-start.1
  5.3 0.7 copy-start.3

commit v3 on v2

--- a/solution.py
+++ b/solution.py
@@ -236,8 +236,6 @@
     if nz > 1:
         forward(1)
     lax.fori_loop(middle, s + 1, key_step, 0)
-    for k in range(2, nz - 1):
-        forward(k)
     parts = []
     for h in range(heads):
         head_out = (weighted[h] / row_sum[h]).astype(jnp.bfloat16)
@@ -251,8 +249,8 @@
     rows, width = resid_ref.shape
     for k in range(1, tp):
         start(part_ref.at[(t + k) % tp], rs_in.at[k], a_s.at[k], a_r.at[k], tdev[k])
-    if nz > 2:
-        forward(nz - 1)
+    for k in range(2, nz - 1):
+        forward(k)
     total = resid_ref[...].astype(jnp.float32)
     mixed = part_ref[t].astype(jnp.float32)
     for k in range(1, tp):
@@ -325,6 +323,8 @@
                     remote(slot, slot, sy.at[k, j], ry.at[k, j], ydev[j]).wait_recv()
 
     gather_step(0)
+    if nz > 2:
+        forward(nz - 1)
     for k in range(nz):
         if k + 1 < nz:
             gather_step(k + 1)
@@ -332,13 +332,16 @@
         if k == 0:
             weights_here()
         compute_step(k)
-        if k >= 1:
+        if k >= 2:
             core_sum(k - 1)
-        if k >= 2:
+        if k >= 3:
             cross_sum(k - 2)
-    core_sum(nz - 1)
-    for k in range(max(nz - 2, 0), nz):
+    if nz > 1:
+        core_sum(nz - 1)
+    core_sum(0)
+    for k in range(max(nz - 2, 1), nz):
         cross_sum(k)
+    cross_sum(0)
     final = after[...].astype(jnp.float32)
     ffn = zsend[0].astype(jnp.float32)
     for k in range(1, nz):

time: 154 us -> 147 us (0.955)
  Pallas kernels: 146 us -> 138 us
    pallas_call x1, Pallas kernels: 146 us -> 138 us  [layer(): pl.pallas_call(functools.partial(layer_kernel, ny, nz, nx), out_shape=jax...]
where the time goes in v3:
time: 147 us; the launch traced here: 146 us
  Pallas kernels  138 us (94%)
  other arithmetic  4.12 us (3%)
  local copies, waits for them, and re-layouts  3.54 us (2%)
    pallas_call x1, Pallas kernels, layer(): pl.pallas_call(functools.partial(layer_kernel, ny, nz, nx), out_shape=jax...  138 us
    unnamed x15, local copies, waits for them, and re-layouts  3.14 us

profile of v3, /device:TPU:0, one launch (start us, length us, event | category | flops | bytes accessed | tf_op | source)
XLA Modules:
  0.0 146.4 jit_solution(16965621735946504170)
XLA Ops:
  0.0 0.0 copy-start
  0.0 0.0 copy-start.2
  0.0 0.8 convert_element_type.36
  0.8 0.1 multiply_cosine_fusion
  1.0 0.0 copy-start.5
  1.0 1.2 fusion
  2.2 0.0 copy-done
  2.2 0.0 copy-done.2
  2.2 0.0 copy-done.5
  2.2 0.0 copy-start.4
  2.2 0.4 fusion.15
  2.6 0.5 copy-done.4
  3.2 0.4 fusion.17
  3.6 0.1 copy.31
  3.7 0.1 copy.34
  3.9 0.1 copy.33
  4.0 0.1 copy.35
  4.2 0.1 fusion.14
  4.2 0.0 copy-start.1
  4.2 0.8 pad_maximum_fusion.q_ref
  5.1 0.1 copy.29
  5.2 0.0 copy-done.1
  5.2 0.1 fusion.4
  5.3 0.0 copy-start.3
  5.4 0.7 copy-done.3
  6.0 0.1 fusion.6
  6.2 0.8 fusion.10.lat_ref
  6.9 137.9 %layer.1 = bf16[64,2048]{1,0:T(8,128)(2,1)} custom-call(bf16[256,640]{1,0:T(8,128)(2,1)} %fusion.10.lat_ref, bf16[4,256,256]{2,1,0:T(8,128)(2,1)} %pad_maximum_fusion.q_ref, bf16[512,256]{1,0:T(8,128)(2,1)} %wks_ref.1, bf16[512,512]{1,0:T(8,128)(2,1)} %wkl_ref.1, bf16[128,2048]{1,0:T(8,128)(2,1)} %wos_ref.1, bf16[256,2048]{1,0:T(8,128)(2,1)} %wol_ref.1, ...), custom_call_target="tpu_custom_call" | custom-call | tf_op jit(solution)/shard_map/layer/pallas_call | solution.py:368
  144.8 1.7 %copy.37 = bf16[64,2048]{1,0:T(8,128)(2,1)} copy(bf16[64,2048]{1,0:T(8,128)(2,1)} %layer.1) | data formatting | bytes 524288
  (10 shorter events, 0.1 us)
Async XLA Ops:
  0.0 2.2 %copy-start = (bf16[768,320]{0,1:T(8,128)(2,1)S(1)}, bf16[768,320]{0,1:T(8,128)(2,1)}, u32[]{:S(2)}) copy-start(bf16[768,320]{0,1:T(8,128)(2,1)} %param.22) | copy-start | bytes 1474564
  0.0 2.2 %copy-start.2 = (bf16[256,768]{1,0:T(8,128)(2,1)S(1)}, bf16[256,768]{1,0:T(8,128)(2,1)}, u32[]{:S(2)}) copy-start(bf16[256,768]{1,0:T(8,128)(2,1)} %param.16) | copy-start | bytes 1179652
  1.0 1.2 copy-start.5
  2.2 1.0 copy-start.4
  4.2 1.0 copy-start.1
  5.3 0.7 copy-start.3
